TPU v7x, 32 devices: a whole 2x2x4 slice. The times are simulated.
32 devices in a mesh: kv: 8 (over z, y), tp: 4 (over x, core).
Axes of the slice: x: 2, y: 2, z: 4, core: 2. Of those that a mesh axis runs over, the one named last changes fastest.
Arguments:
- tokens: bfloat16 [4, 4096], P(None, 'kv'), may hold values from -70 to 70
- norm_gain: float32 [4096], P('kv'), may hold values from 0.1 to 1.9
- query_weight: bfloat16 [4096, 2048], P('kv', 'tp'), may hold values from -0.09375 to 0.09375
- key_weight: bfloat16 [4096, 256], P('kv', 'tp'), may hold values from -0.09375 to 0.09375
- value_weight: bfloat16 [4096, 256], P('kv', 'tp'), may hold values from -0.09375 to 0.09375
- cache_keys: bfloat16 [4, 2, 6144, 128], P(None, None, ('kv', 'tp')), may hold values from -480 to 480, as said below
- cache_values: bfloat16 [4, 2, 6144, 128], P(None, None, ('kv', 'tp')), may hold values from -6 to 6
- lengths: int32 [4], replicated, may hold values from 1536 to 6143
- lambdas: float32 [16], P('tp'), may hold values from 0.3 to 0.8
- head_gain: float32 [128], replicated, may hold values from 0.1 to 1.9
- output_weight: bfloat16 [2048, 4096], P('tp', 'kv'), may hold values from -0.125 to 0.125
Outputs:
- attended: bfloat16 [4, 4096], P(None, 'kv')
- new_keys: bfloat16 [4, 256], P(None, 'tp')
- new_values: bfloat16 [4, 256], P(None, 'tp')
Inputs may be any that keep to these rules, and one draw needn't show every extreme that they name: `cache_keys`: of order 1.75 in most entries; some rows may be far larger.
All inputs are finite; a program needn't handle non-finite values.
Results may differ from a plain program's by a relative error of at most 0.038.
Values may be sent and summed in bfloat16 or wider, within the bound.
No kernel may reach another device: no remote copies, remote signals or barrier semaphores. Data moves between devices by JAX's collectives and lax.ppermute only.
A program may use at most 64 MiB of HBM per device.

v0:
```python
import jax
import jax.numpy as jnp
from jax import lax
from jax.sharding import PartitionSpec as P

D = 4096
HEADS = 16
KV_HEADS = 2
QK = 64
VD = 128
NEG_FILL = -1e30


def body(
    tokens,
    norm_gain,
    query_weight,
    key_weight,
    value_weight,
    cache_keys,
    cache_values,
    lengths,
    lambdas,
    head_gain,
    output_weight,
):
    floats = tokens.astype(jnp.float32)
    scaled = (floats * norm_gain).astype(jnp.bfloat16)
    query_part = jnp.dot(scaled, query_weight, preferred_element_type=jnp.float32)
    key_part = jnp.dot(scaled, key_weight, preferred_element_type=jnp.float32)
    value_part = jnp.dot(scaled, value_weight, preferred_element_type=jnp.float32)
    squares, query_sum, key_sum, value_sum = lax.psum(
        (jnp.sum(floats * floats, axis=1), query_part, key_part, value_part), "kv"
    )
    inverse = lax.rsqrt(squares / D + 1e-06)[:, None]
    queries = (query_sum * inverse).astype(jnp.bfloat16)
    new_keys = (key_sum * inverse).astype(jnp.bfloat16)
    new_values = (value_sum * inverse).astype(jnp.bfloat16)
    every_query = lax.all_gather(queries, "tp", axis=1, tiled=True)
    seq_count = tokens.shape[0]
    pos_count = cache_keys.shape[2]
    group_size = HEADS // KV_HEADS
    own_heads = lambdas.shape[0]
    first_position = (lax.axis_index("kv") * lax.axis_size("tp") + lax.axis_index("tp")) * pos_count
    positions = first_position + jnp.arange(pos_count, dtype=jnp.int32)
    live_mask = (positions[None, :] < lengths[:, None])[:, None, None, None, :]
    query_rows = every_query.reshape(seq_count, KV_HEADS, group_size, 2, QK)
    key_rows = cache_keys.reshape(seq_count, KV_HEADS, pos_count, 2, QK)
    scores = jnp.einsum(
        "bhgcd,bhpcd->bhgcp", query_rows, key_rows, preferred_element_type=jnp.float32
    ) * QK ** (-0.5)
    scores = jnp.where(live_mask, scores, NEG_FILL)
    local_peak = jnp.max(scores, axis=-1)
    peak_used = lax.pmax(local_peak, ("kv", "tp"))
    weights = jnp.where(live_mask, jnp.exp(scores - peak_used[..., None]), 0.0)
    totals = jnp.sum(weights, axis=-1).reshape(seq_count, HEADS, 2)
    summed = jnp.einsum(
        "bhgcp,bhpv->bhgcv",
        weights.astype(jnp.bfloat16),
        cache_values,
        preferred_element_type=jnp.float32,
    ).reshape(seq_count, HEADS, 2, VD)
    totals, summed = (
        lax.psum_scatter(totals.astype(jnp.bfloat16), "tp", scatter_dimension=1, tiled=True).astype(
            jnp.float32
        ),
        lax.psum_scatter(summed.astype(jnp.bfloat16), "tp", scatter_dimension=1, tiled=True).astype(
            jnp.float32
        ),
    )
    totals, summed = lax.psum((totals, summed), "kv")
    ratios = summed / totals[..., None]
    mixed = ratios[:, :, 0] - lambdas[None, :, None] * ratios[:, :, 1]
    normed = mixed * lax.rsqrt(jnp.mean(mixed * mixed, axis=-1, keepdims=True) + 1e-06) * head_gain
    flattened = normed.astype(jnp.bfloat16).reshape(seq_count, own_heads * VD)
    partial_out = jnp.dot(flattened, output_weight, preferred_element_type=jnp.float32)
    attended = lax.psum(partial_out.astype(jnp.bfloat16), "tp")
    return (attended, new_keys, new_values)


def solution(mesh):
    return jax.shard_map(
        body,
        mesh=mesh,
        in_specs=(
            P(None, "kv"),
            P("kv"),
            P("kv", "tp"),
            P("kv", "tp"),
            P("kv", "tp"),
            P(None, None, ("kv", "tp"), None),
            P(None, None, ("kv", "tp"), None),
            P(),
            P("tp"),
            P(),
            P("tp", "kv"),
        ),
        out_specs=(P(None, "kv"), P(None, "tp"), P(None, "tp")),
        check_vma=False,
    )
```

profile of v0, /device:TPU:0, one launch (start us, length us, event | category | flops | bytes accessed | tf_op | source)
XLA Modules:
  0.0 127.6 jit_solution(1251713564693285807)
XLA Ops:
  0.6 0.0 copy-start
  0.6 0.0 copy-start.2
  0.7 0.8 broadcast_compare_fusion
  1.5 0.2 copy-done
  1.7 0.0 copy-start.3
  1.7 0.9 fusion.24
  2.6 0.0 copy-done.3
  2.6 0.1 fusion.11
  2.8 23.6 %all-reduce.3 = (f32[4,512]{1,0:T(4,128)S(1)}, f32[4]{0:T(128)S(1)}) all-reduce(f32[4,512]{1,0:T(4,128)S(1)} %fusion.24, f32[4]{0:T(128)S(1)} %fusion.11), channel_id=1, replica_groups=mesh['kv'=8,'tp'=4] {'kv'}, use_global_device_ids=true, to_apply=%region_0.0 | all-reduce | flops 2052 | bytes 16416 | tf_op jit(solution)/shard_map/psum | solution.py:32
  26.4 0.1 multiply_convert_fusion
  26.5 5.2 %all_gather.3 = bf16[4,2048]{1,0:T(4,128)(2,1)S(1)} all-gather(bf16[4,512]{1,0:T(4,128)(2,1)S(1)} %multiply_convert_fusion), channel_id=1, replica_groups=mesh['kv'=8,'tp'=4] {'tp'}, dimensions={1}, use_global_device_ids=true | all-gather | bytes 20480 | tf_op jit(solution)/shard_map/all_gather | solution.py:39
  31.7 0.1 reshape.63
  31.8 0.0 copy-done.2
  31.8 0.2 copy.22
  32.0 0.0 copy-start.9
  32.0 0.3 fusion.27
  32.3 36.9 %pmax.7 = f32[4,2,8,2]{2,3,1,0:T(2,128)S(1)} all-reduce(f32[4,2,8,2]{2,3,1,0:T(2,128)S(1)} %get-tuple-element.15), channel_id=1, replica_groups=mesh['kv'=8,'tp'=4] {'kv','tp'}, use_global_device_ids=true, to_apply=%region_4.0 | all-reduce | flops 128 | bytes 1024 | tf_op jit(solution)/shard_map/pmax | solution.py:54
  69.2 0.2 fusion.3
  69.4 0.1 convert_element_type.51
  69.5 0.0 copy-done.9
  69.5 0.0 copy-start.1
  69.5 0.3 convolution_convert_fusion
  69.7 0.0 copy-start.10
  69.8 0.0 copy-start.4
  69.8 0.0 copy-start.6
  69.8 11.5 %all-reduce.4 = (bf16[4,16,2,128]{3,1,2,0:T(8,128)(2,1)S(1)}, bf16[4,16,2]{1,2,0:T(2,128)(2,1)S(1)}) all-reduce(bf16[4,16,2,128]{3,1,2,0:T(8,128)(2,1)S(1)} %bitcast.69, bf16[4,16,2]{1,2,0:T(2,128)(2,1)S(1)} %convert_element_type.51), channel_id=2, replica_groups=mesh['kv'=8,'tp'=4] {'tp'}, use_global_device_ids=true, to_apply=%region_5.6.clone | all-reduce | flops 16512 | bytes 66048
  81.3 0.0 copy-start.5
  81.4 0.0 copy-done.10
  81.4 0.6 dynamic-slice
  82.6 0.1 dynamic-slice_convert_fusion.1
  82.7 0.0 copy-done.4
  82.7 0.0 copy-done.6
  82.7 0.1 fusion.20
  82.8 0.0 copy-done.5
  82.8 0.1 fusion.22
  83.0 35.9 %all-reduce.2 = (f32[4,4,2,128]{3,1,2,0:T(4,128)S(1)}, f32[4,4,2]{1,2,0:T(2,128)S(1)}, f32[4,64]{1,0:T(4,128)S(1)}, f32[4,64]{1,0:T(4,128)S(1)}) all-reduce(f32[4,4,2,128]{3,1,2,0:T(4,128)S(1)} %dynamic-slice_convert_fusion, f32[4,4,2]{1,2,0:T(2,128)S(1)} %dynamic-slice_convert_fusion.1, ...), channel_id=1, replica_groups=mesh['kv'=8,'tp'=4] {'kv'}, use_global_device_ids=true, to_apply=%region_6.7 | all-reduce | flops 4640 | bytes 37120 | tf_op jit(solution)/shard_map/psum | solution.py:71
  118.9 0.6 multiply_convert_fusion.1
  119.5 0.1 broadcast_divide_fusion
  119.6 0.0 copy-start.7
  119.7 0.6 copy-done.7
  120.3 0.2 fusion.16
  120.5 0.0 copy-start.8
  120.5 0.1 broadcast_bitcast_fusion
  120.5 0.6 copy-done.8
  121.1 0.1 broadcast_bitcast_fusion.1
  121.2 0.0 copy-done.1
  121.2 0.2 convolution_convert_fusion.1
  121.4 6.2 %psum.53 = bf16[4,512]{1,0:T(4,128)(2,1)} all-reduce(bf16[4,512]{1,0:T(4,128)(2,1)S(1)} %convolution_convert_fusion.1), channel_id=1, replica_groups=mesh['kv'=8,'tp'=4] {'tp'}, use_global_device_ids=true, to_apply=%region_11.12 | all-reduce | flops 2048 | bytes 8192 | tf_op jit(solution)/shard_map/psum | solution.py:77
  (7 shorter events, 0.1 us)
Async XLA Ops:
  0.6 1.1 copy-start
  0.6 31.1 %copy-start.2 = (bf16[4,2,192,128]{3,2,1,0:T(8,128)(2,1)S(1)}, bf16[4,2,192,128]{3,2,1,0:T(8,128)(2,1)}, u32[]{:S(2)}) copy-start(bf16[4,2,192,128]{3,2,1,0:T(8,128)(2,1)} %param.16) | copy-start | bytes 1179652
  1.7 0.9 copy-start.3
  32.0 37.5 %copy-start.9 = (bf16[4,2,192,128]{3,2,1,0:T(8,128)(2,1)S(1)}, bf16[4,2,192,128]{3,2,1,0:T(8,128)(2,1)}, u32[]{:S(2)}) copy-start(bf16[4,2,192,128]{3,2,1,0:T(8,128)(2,1)} %param.17) | copy-start | bytes 1179652
  69.5 51.7 %copy-start.1 = (bf16[512,512]{1,0:T(8,128)(2,1)S(1)}, bf16[512,512]{1,0:T(8,128)(2,1)}, u32[]{:S(2)}) copy-start(bf16[512,512]{1,0:T(8,128)(2,1)} %param.21) | copy-start | bytes 1572868
  69.7 11.6 %copy-start.10 = (u32[32]{0:T(128)S(1)}, u32[32]{0:T(128)}, u32[]{:S(2)}) copy-start(u32[32]{0:T(128)} %constant.32) | copy-start | bytes 388
  69.8 12.9 %copy-start.4 = (bf16[512,64]{0,1:T(8,128)(2,1)S(1)}, bf16[512,64]{0,1:T(8,128)(2,1)}, u32[]{:S(2)}) copy-start(bf16[512,64]{0,1:T(8,128)(2,1)} %param.15) | copy-start | bytes 196612
  69.8 12.9 %copy-start.6 = (f32[512]{0:T(512)S(1)}, f32[512]{0:T(512)}, u32[]{:S(2)}) copy-start(f32[512]{0:T(512)} %param.12) | copy-start | bytes 6148
  81.3 1.5 %copy-start.5 = (bf16[512,64]{0,1:T(8,128)(2,1)S(1)}, bf16[512,64]{0,1:T(8,128)(2,1)}, u32[]{:S(2)}) copy-start(bf16[512,64]{0,1:T(8,128)(2,1)} %param.14) | copy-start | bytes 196612
  119.6 0.7 copy-start.7
  120.5 0.7 copy-start.8
where the time goes:
time: 128 us
  blocking collectives  119 us (93%)
  local copies, waits for them, and re-layouts  2.65 us (2%)
  other arithmetic  2.17 us (2%)
  matrix products  1.87 us (1%)
  between operations  1.46 us (1%)
    pmax x1, blocking collectives, body(): peak_used = lax.pmax(local_peak, ('kv', 'tp'))  36.9 us
    psum x1, blocking collectives, body(): totals, summed = lax.psum((totals, summed), 'kv')  35.9 us
    psum x1, blocking collectives, body(): lax.psum((jnp.sum(floats * floats, axis=1), query_part, key_part, value_p...  23.6 us
    unnamed x1, blocking collectives  11.5 us
    psum x1, blocking collectives, body(): attended = lax.psum(partial_out.astype(jnp.bfloat16), 'tp')  6.24 us
    all_gather x1, blocking collectives, body(): every_query = lax.all_gather(queries, 'tp', axis=1, tiled=True)  5.19 us

commit v1 on v0

--- a/solution.py
+++ b/solution.py
@@ -36,7 +36,9 @@
     queries = (query_sum * inverse).astype(jnp.bfloat16)
     new_keys = (key_sum * inverse).astype(jnp.bfloat16)
     new_values = (value_sum * inverse).astype(jnp.bfloat16)
-    every_query = lax.all_gather(queries, "tp", axis=1, tiled=True)
+    every_query = jnp.concatenate(
+        lax.all_to_all(jnp.stack([queries] * lax.axis_size("tp")), "tp", 0, 0), axis=1
+    )
     seq_count = tokens.shape[0]
     pos_count = cache_keys.shape[2]
     group_size = HEADS // KV_HEADS

time: 128 us -> 127 us (level)
  blocking collectives: 119 us -> 114 us
  starting transfers between devices: 0 us -> 3.38 us
    all_gather x1 -> x0, blocking collectives: 5.19 us -> none  [body(): every_query = lax.all_gather(queries, 'tp', axis=1, tiled=True)]
    all_to_all x0 -> x1, starting transfers between devices: none -> 3.38 us  [body(): lax.all_to_all(jnp.stack([queries] * lax.axis_size('tp')), 'tp', 0, 0)]
    unnamed x26 -> x28, local copies, waits for them, and re-layouts: 2.37 us -> 2.86 us
  transfers between devices with their start and end apart: 0 -> 1, of which waited for: 0 -> 1; matrix products, arithmetic and copies ran while one was open for 0% -> 1% of each run, Pallas kernels for 0% -> 0%
where the time goes in v1:
time: 127 us
  blocking collectives  114 us (90%)
  local copies, waits for them, and re-layouts  3.74 us (3%)
  starting transfers between devices  3.38 us (3%)
  other arithmetic  2.19 us (2%)
  matrix products  1.86 us (1%)
  between operations  1.47 us (1%)
    pmax x1, blocking collectives, body(): peak_used = lax.pmax(local_peak, ('kv', 'tp'))  36.9 us
    psum x1, blocking collectives, body(): totals, summed = lax.psum((totals, summed), 'kv')  35.6 us
    psum x1, blocking collectives, body(): lax.psum((jnp.sum(floats * floats, axis=1), query_part, key_part, value_p...  23.6 us
    unnamed x1, blocking collectives  11.7 us
    psum x1, blocking collectives, body(): attended = lax.psum(partial_out.astype(jnp.bfloat16), 'tp')  6.24 us
    all_to_all x1, starting transfers between devices, body(): lax.all_to_all(jnp.stack([queries] * lax.axis_size('tp')), 'tp', 0, 0)  3.38 us
    unnamed x28, local copies, waits for them, and re-layouts  2.86 us
  transfers between devices with their start and end apart: 1, of which 1 were waited for; matrix products, arithmetic and copies ran while one was open for 1% of the time, Pallas kernels for 0%

profile of v1, /device:TPU:0, one launch (start us, length us, event | category | flops | bytes accessed | tf_op | source)
XLA Modules:
  0.0 126.9 jit_solution(10512281158984263683)
XLA Ops:
  0.6 0.0 copy-start
  0.6 0.0 copy-start.3
  0.7 0.9 fusion.11
  1.5 0.2 copy-done
  1.7 0.0 copy-done.3
  1.7 0.0 copy-start.2
  1.7 0.9 fusion.24
  2.6 0.0 copy-start.4
  2.6 23.6 %all-reduce.3 = (f32[4,512]{1,0:T(4,128)S(1)}, f32[4]{0:T(128)S(1)}) all-reduce(f32[4,512]{1,0:T(4,128)S(1)} %fusion.24, f32[4]{0:T(128)S(1)} %fusion.11), channel_id=1, replica_groups=mesh['kv'=8,'tp'=4] {'kv'}, use_global_device_ids=true, to_apply=%region_0.0 | all-reduce | flops 2052 | bytes 16416 | tf_op jit(solution)/shard_map/psum | solution.py:32
  26.3 0.1 multiply_convert_fusion
  26.3 0.0 copy-start.6
  26.3 0.6 stack.2
  26.9 3.4 %all-to-all-start = ((bf16[4,4,512]{2,1,0:T(4,128)(2,1)}), bf16[4,4,512]{2,1,0:T(4,128)(2,1)S(1)}, u32[]{:S(2)}, u32[]{:S(2)}) async-start(bf16[4,4,512]{2,1,0:T(4,128)(2,1)} %stack.2), calls=%async_computation | async-start | bytes 32768 | tf_op jit(solution)/shard_map/all_to_all | solution.py:40
  30.3 0.0 copy-done.4
  30.4 0.0 copy-done.6
  30.4 0.1 fusion.20
  30.5 0.0 copy-done.5
  30.5 0.1 fusion.22
  30.6 0.5 copy-done.7
  31.2 0.0 copy-done.8
  31.2 0.1 broadcast_bitcast_fusion.1
  31.3 0.6 copy-done.9
  31.8 0.1 broadcast_compare_fusion
  31.9 0.0 copy-done.2
  31.9 0.2 copy.22
  32.1 0.0 copy-start.11
  32.1 0.6 copy-done.11
  32.8 0.6 dynamic-slice
  34.0 0.1 all-to-all-done
  34.2 0.1 reshape_reshape.3
  34.3 0.0 copy-start.10
  34.3 0.3 fusion.27
  34.5 36.9 %pmax.7 = f32[4,2,8,2]{2,3,1,0:T(2,128)S(1)} all-reduce(f32[4,2,8,2]{2,3,1,0:T(2,128)S(1)} %get-tuple-element.15), channel_id=1, replica_groups=mesh['kv'=8,'tp'=4] {'kv','tp'}, use_global_device_ids=true, to_apply=%region_4.0 | all-reduce | flops 128 | bytes 1024 | tf_op jit(solution)/shard_map/pmax | solution.py:56
  71.4 0.2 fusion.3
  71.6 0.0 copy-start.1
  71.7 0.1 convert_element_type.51
  71.7 0.0 copy-done.10
  71.8 0.3 convolution_convert_fusion
  72.0 11.7 %all-reduce.4 = (bf16[4,16,2,128]{3,1,2,0:T(8,128)(2,1)S(1)}, bf16[4,16,2]{1,2,0:T(2,128)(2,1)S(1)}) all-reduce(bf16[4,16,2,128]{3,1,2,0:T(8,128)(2,1)S(1)} %bitcast.70, bf16[4,16,2]{1,2,0:T(2,128)(2,1)S(1)} %convert_element_type.51), channel_id=2, replica_groups=mesh['kv'=8,'tp'=4] {'tp'}, use_global_device_ids=true, to_apply=%region_5.6.clone | all-reduce | flops 16512 | bytes 66048
  83.8 0.1 dynamic-slice_convert_fusion.1
  83.9 35.6 %all-reduce.2 = (f32[4,4,2,128]{3,1,2,0:T(4,128)S(1)}, f32[4,4,2]{1,2,0:T(2,128)S(1)}, f32[4,64]{1,0:T(4,128)S(1)}, f32[4,64]{1,0:T(4,128)S(1)}) all-reduce(f32[4,4,2,128]{3,1,2,0:T(4,128)S(1)} %dynamic-slice_convert_fusion, f32[4,4,2]{1,2,0:T(2,128)S(1)} %dynamic-slice_convert_fusion.1, ...), channel_id=1, replica_groups=mesh['kv'=8,'tp'=4] {'kv'}, use_global_device_ids=true, to_apply=%region_6.7 | all-reduce | flops 4640 | bytes 37120 | tf_op jit(solution)/shard_map/psum | solution.py:73
  119.5 0.1 broadcast_divide_fusion
  119.6 0.2 fusion.16
  119.8 0.1 broadcast_bitcast_fusion
  119.8 0.0 copy-done.1
  119.9 0.2 convolution_convert_fusion.1
  120.0 6.2 %psum.53 = bf16[4,512]{1,0:T(4,128)(2,1)} all-reduce(bf16[4,512]{1,0:T(4,128)(2,1)S(1)} %convolution_convert_fusion.1), channel_id=1, replica_groups=mesh['kv'=8,'tp'=4] {'tp'}, use_global_device_ids=true, to_apply=%region_11.12 | all-reduce | flops 2048 | bytes 8192 | tf_op jit(solution)/shard_map/psum | solution.py:79
  126.3 0.6 multiply_convert_fusion.1
  (12 shorter events, 0.1 us)
Async XLA Ops:
  0.6 1.1 copy-start
  0.6 1.1 copy-start.3
  1.7 30.2 %copy-start.2 = (bf16[4,2,192,128]{3,2,1,0:T(8,128)(2,1)S(1)}, bf16[4,2,192,128]{3,2,1,0:T(8,128)(2,1)}, u32[]{:S(2)}) copy-start(bf16[4,2,192,128]{3,2,1,0:T(8,128)(2,1)} %param.16) | copy-start | bytes 1179652
  2.6 27.8 %copy-start.4 = (bf16[512,64]{0,1:T(8,128)(2,1)S(1)}, bf16[512,64]{0,1:T(8,128)(2,1)}, u32[]{:S(2)}) copy-start(bf16[512,64]{0,1:T(8,128)(2,1)} %param.15) | copy-start | bytes 196612
  26.3 4.0 %copy-start.6 = (f32[512]{0:T(512)S(1)}, f32[512]{0:T(512)}, u32[]{:S(2)}) copy-start(f32[512]{0:T(512)} %param.12) | copy-start | bytes 6148
  26.9 3.6 %copy-start.5 = (bf16[512,64]{0,1:T(8,128)(2,1)S(1)}, bf16[512,64]{0,1:T(8,128)(2,1)}, u32[]{:S(2)}) copy-start(bf16[512,64]{0,1:T(8,128)(2,1)} %param.14) | copy-start | bytes 196612
  26.9 7.2 %all-to-all-start = ((bf16[4,4,512]{2,1,0:T(4,128)(2,1)}), bf16[4,4,512]{2,1,0:T(4,128)(2,1)S(1)}, u32[]{:S(2)}, u32[]{:S(2)}) async-start(bf16[4,4,512]{2,1,0:T(4,128)(2,1)} %stack.2), calls=%async_computation | async-start | bytes 32768 | tf_op jit(solution)/shard_map/all_to_all | solution.py:40
  30.5 0.7 copy-start.7
  30.5 0.7 copy-start.8
  31.2 0.7 copy-start.9
  32.1 0.7 copy-start.11
  34.3 37.5 %copy-start.10 = (bf16[4,2,192,128]{3,2,1,0:T(8,128)(2,1)S(1)}, bf16[4,2,192,128]{3,2,1,0:T(8,128)(2,1)}, u32[]{:S(2)}) copy-start(bf16[4,2,192,128]{3,2,1,0:T(8,128)(2,1)} %param.17) | copy-start | bytes 1179652
  71.6 48.2 %copy-start.1 = (bf16[512,512]{1,0:T(8,128)(2,1)S(1)}, bf16[512,512]{1,0:T(8,128)(2,1)}, u32[]{:S(2)}) copy-start(bf16[512,512]{1,0:T(8,128)(2,1)} %param.21) | copy-start | bytes 1572868
